TPU v7x, 32 devices: a whole 2x2x4 slice. The times are simulated.
32 devices in a mesh: sp: 8 (over z, x), tp: 4 (over y, core).
Axes of the slice: x: 2, y: 2, z: 4, core: 2. Of those that a mesh axis runs over, the one named last changes fastest.
Arguments:
- residual: bfloat16 [2048, 2048], P('sp', 'tp'), may hold values from -48 to 48
- queries: bfloat16 [2048, 1024], P('sp', 'tp'), may hold values from -6 to 6
- key_rows: bfloat16 [2048, 512], P('sp', 'tp'), may hold values from -6 to 6
- value_rows: bfloat16 [2048, 512], P('sp', 'tp'), may hold values from -6 to 6
- break_shift: bfloat16 [4, 2048], P('tp', 'sp'), may hold values from -20 to 0
- head_gain: float32 [1024], P('tp'), may hold values from 0.1 to 1.9
- out_weight: bfloat16 [1024, 2048], P('tp'), may hold values from -0.1875 to 0.1875
- mlp_gain: float32 [2048], replicated, may hold values from 0.1 to 1.9
- up_weight: bfloat16 [2048, 8192], P('sp', 'tp'), may hold values from -0.125 to 0.125
- down_weight: bfloat16 [8192, 2048], P('tp', 'sp'), may hold values from -0.0625 to 0.0625
Outputs:
- layer_out: bfloat16 [2048, 2048], P('sp', 'tp')
All inputs are finite; a program needn't handle non-finite values.
Results may differ from a plain program's by a relative error of at most 0.013.
Values may be sent and summed in bfloat16 or wider, within the bound.
A program may use at most 128 MiB of HBM per device.

v0:
```python
import jax
import jax.numpy as jnp
from jax import lax
from jax.sharding import PartitionSpec as P

HEAD_DIM = 128
eps = 1e-06


def stick_attention(queries, key_all, value_all, shift_all, first_pos, key_block):
    token_count = queries.shape[0]
    kv_local = key_all.shape[1] // HEAD_DIM
    query_local = queries.shape[1] // HEAD_DIM
    group_size = query_local // kv_local
    stacked = queries.reshape(token_count, kv_local, group_size, HEAD_DIM).transpose(1, 2, 0, 3)
    stacked = stacked.reshape(kv_local, group_size * token_count, HEAD_DIM)
    query_pos = first_pos + lax.iota(jnp.int32, group_size * token_count) % token_count
    score_scale = HEAD_DIM ** (-0.5)
    block_count = (first_pos + token_count - 1 + key_block - 1) // key_block

    def one_block(turn_index, state_pair):
        running, broken_after = state_pair
        offset = (block_count - 1 - turn_index) * key_block
        key_block_rows = lax.dynamic_slice_in_dim(key_all, offset, key_block, 0).reshape(
            key_block, kv_local, HEAD_DIM
        )
        value_block_rows = lax.dynamic_slice_in_dim(value_all, offset, key_block, 0).reshape(
            key_block, kv_local, HEAD_DIM
        )
        shift_block = lax.dynamic_slice_in_dim(shift_all, offset, key_block, 1).astype(jnp.float32)
        scores = jnp.einsum(
            "grd,kgd->grk", stacked, key_block_rows, preferred_element_type=jnp.float32
        )
        scores = scores * score_scale + shift_block[:, None, :]
        key_pos = offset + lax.iota(jnp.int32, key_block)
        visible = key_pos[None, None, :] < query_pos[None, :, None]
        broken = jnp.where(visible, jax.nn.log_sigmoid(-scores), 0.0)
        later = lax.cumsum(broken, axis=2, reverse=True) - broken + broken_after[:, :, None]
        weights = jnp.where(visible, jnp.exp(jax.nn.log_sigmoid(scores) + later), 0.0).astype(
            jnp.bfloat16
        )
        running = running + jnp.einsum(
            "grk,kgd->grd", weights, value_block_rows, preferred_element_type=jnp.float32
        )
        return (running, broken_after + jnp.sum(broken, axis=2))

    start_pair = (
        jnp.zeros((kv_local, group_size * token_count, HEAD_DIM), jnp.float32),
        jnp.zeros((kv_local, group_size * token_count), jnp.float32),
    )
    running, broken_after = lax.fori_loop(0, block_count, one_block, start_pair)
    running = running.reshape(kv_local, group_size, token_count, HEAD_DIM).transpose(2, 0, 1, 3)
    return running.reshape(token_count, query_local, HEAD_DIM)


def body(
    residual,
    queries,
    key_rows,
    value_rows,
    break_shift,
    head_gain,
    out_weight,
    mlp_gain,
    up_weight,
    down_weight,
):
    token_count = queries.shape[0]
    first_pos = lax.axis_index("sp") * token_count
    key_all, value_all, shift_all = (
        lax.all_gather(key_rows, "sp", axis=0, tiled=True),
        lax.all_gather(value_rows, "sp", axis=0, tiled=True),
        lax.all_gather(break_shift, "sp", axis=1, tiled=True),
    )
    key_block = min(2048, key_all.shape[0])
    mixed = stick_attention(queries, key_all, value_all, shift_all, first_pos, key_block)
    power = jnp.mean(mixed * mixed, axis=2, keepdims=True)
    attended = (mixed * lax.rsqrt(power + eps) * head_gain.reshape(-1, HEAD_DIM)).astype(
        jnp.bfloat16
    )
    attended = attended.reshape(token_count, -1)
    partial_value = jnp.dot(attended, out_weight, preferred_element_type=jnp.float32)
    column_count = residual.shape[1]
    column_start = lax.axis_index("tp") * column_count
    own_part = lax.dynamic_slice_in_dim(
        partial_value, column_start, column_count, 1
    ) + residual.astype(jnp.float32)
    partial_value = lax.dynamic_update_slice_in_dim(partial_value, own_part, column_start, 1)
    hidden_whole = lax.psum(partial_value, "tp").astype(jnp.bfloat16)
    widened = hidden_whole.astype(jnp.float32)
    inverse = lax.rsqrt(jnp.mean(widened * widened, axis=1, keepdims=True) + eps)
    mlp_in = (widened * inverse * mlp_gain).astype(jnp.bfloat16)
    hidden_state = lax.dynamic_slice_in_dim(hidden_whole, column_start, column_count, 1)
    lifted = jnp.dot(
        mlp_in,
        lax.all_gather(up_weight, "sp", axis=0, tiled=True),
        preferred_element_type=jnp.float32,
    )
    activated = jnp.square(jax.nn.relu(lifted)).astype(jnp.bfloat16)
    expanded = jnp.dot(
        activated,
        lax.all_gather(down_weight, "sp", axis=1, tiled=True),
        preferred_element_type=jnp.float32,
    )
    mlp_total = lax.psum_scatter(
        expanded.astype(jnp.bfloat16), "tp", scatter_dimension=1, tiled=True
    ).astype(jnp.float32)
    return (hidden_state.astype(jnp.float32) + mlp_total).astype(jnp.bfloat16)


def solution(mesh):
    in_specs = (
        P("sp", "tp"),
        P("sp", "tp"),
        P("sp", "tp"),
        P("sp", "tp"),
        P("tp", "sp"),
        P("tp"),
        P("tp", None),
        P(),
        P("sp", "tp"),
        P("tp", "sp"),
    )
    out_specs = P("sp", "tp")
    return jax.shard_map(body, mesh=mesh, in_specs=in_specs, out_specs=out_specs, check_vma=False)
```

profile of v0, /device:TPU:0, one launch (start us, length us, event | category | flops | bytes accessed | tf_op | source)
XLA Modules:
  0.0 312.5 jit_solution(17928566602720874883)
XLA Ops:
  6.5 0.0 copy-start
  6.5 0.0 all-gather.3.cloned.1.call-start
  6.5 0.7 all-gather.3.cloned.1.call-update
  7.3 0.0 all-gather.5.cloned.1.call-start
  7.3 0.7 all-gather.5.cloned.1.call-update
  8.0 0.0 reduce-scatter.2.cloned.1.call-start
  8.1 35.3 %all_gather.15 = bf16[2048,128]{1,0:T(8,128)(2,1)S(1)} all-gather(bf16[256,128]{1,0:T(8,128)(2,1)} %param.14), channel_id=1, replica_groups=mesh['sp'=8,'tp'=4] {'sp'}, dimensions={0}, use_global_device_ids=true | all-gather | bytes 589824 | tf_op jit(solution)/shard_map/all_gather | solution.py:71
  43.4 33.5 %all_gather.17 = bf16[2048,128]{1,0:T(8,128)(2,1)S(1)} all-gather(bf16[256,128]{1,0:T(8,128)(2,1)} %param.15), channel_id=1, replica_groups=mesh['sp'=8,'tp'=4] {'sp'}, dimensions={0}, use_global_device_ids=true | all-gather | bytes 589824 | tf_op jit(solution)/shard_map/all_gather | solution.py:72
  76.9 0.9 reshape.144
  77.9 22.0 %all_gather.16 = bf16[1,2048]{1,0:T(2,128)(2,1)S(1)} all-gather(bf16[1,256]{1,0:T(2,128)(2,1)} %param.16), channel_id=1, replica_groups=mesh['sp'=8,'tp'=4] {'sp'}, dimensions={1}, use_global_device_ids=true | all-gather | bytes 4608 | tf_op jit(solution)/shard_map/all_gather | solution.py:73
  99.9 0.0 copy-start.3
  99.9 48.2 %while.15 = (s32[]{:T(128)}, f32[1,512,128]{2,1,0:T(8,128)S(1)}, f32[1,512]{1,0:T(1,128)S(1)}, s32[]{:T(128)}, s32[]{:T(128)}, /*index=5*/bf16[1,512,128]{2,1,0:...) while((s32[]{:T(128)}, f32[1,512,128]{2,1,0:T(8,128)S(1)}, ...), condition=%wide.region_4.5_spmd.clone, body=%wide.region_0.4_spmd.clone.sunk | while | flops 709041152 | bytes 81762496 | solution.py:51
  100.0 2.6 fusion.64
  102.6 5.0 %fusion.66 = (f32[512]{0:T(512)S(1)}, f32[64,8,16,128]{3,1,2,0:T(8,128)S(1)}) fusion(f32[2048]{0:T(1024)S(1)} %bitcast.98, f32[512,2048]{1,0:T(8,128)} %fusion.64, s32[512]{0:T(512)S(1)} %fusion.65, s32[2048]{0:T(1024)S(1)} %iota_add_fusion.2), kind=kLoop, calls=%fused_computation.30.clone.1 | loop fusion | flops 12582400 | bytes 8409088 | tf_op jit(solution)/shard_map/while/body/reduce_sum | solution.py:45
  107.7 2.9 copy.47
  110.6 5.6 %copy.48 = f32[1,512,16,128]{1,2,3,0:T(8,128)} copy(f32[1,512,16,128]{3,2,1,0:T(8,128)} %bitcast.92) | data formatting | bytes 8388608 | tf_op jit(solution)/shard_map/reshape.112
  116.2 10.8 %fusion.67 = f32[1,512,16,128]{1,2,3,0:T(8,128)S(1)} fusion(f32[1,512,16,128]{1,2,3,0:T(8,128)} %copy.48), kind=kOutput, calls=%fused_computation.52.clone.1 | output fusion | flops 133169152 | bytes 8388608 | tf_op jit(solution)/shard_map/reduce-window.4
  127.0 0.0 copy-start.1
  127.0 1.9 copy-done.1
  128.9 0.1 reduce-window.20
  129.0 0.1 copy.49
  129.2 2.6 broadcast.100
  131.8 5.8 %copy.50 = f32[1,512,16,128]{3,2,1,0:T(8,128)} copy(f32[1,512,16,128]{1,2,3,0:T(8,128)} %copy-done.1) | data formatting | bytes 8388608 | tf_op jit(solution)/shard_map/reduce-window.4
  137.6 10.4 %fusion.68 = f32[1,512,128]{2,1,0:T(8,128)S(1)} fusion(f32[1,512,128]{2,1,0:T(8,128)S(1)} %get-tuple-element.245, bf16[2048,128]{1,0:T(8,128)(2,1)S(1)} %get-tuple-element.265, f32[64,8,16,128]{3,2,1,0:T(8,128)} %bitcast.93, f32[64,8,16,128]{3,2,1,0:T(8,128)} %bitcast.94, f32[512,2048]{1,0:T(8,128)} %fusion.64, f32[512]{0:T(512)S(1)} %bitcast.101, ...), kind=kOutput, calls=%fused_computation.16.clone.1 | convolution fusion | flops 294715392 | bytes 13651968 | tf_op jit(solution)/shard_map/while/body/grk,kgd->grd/dot_general | solution.py:42
  148.2 0.0 copy-start.2
  148.2 0.1 copy.23
  148.4 0.1 multiply_reduce_fusion
  148.5 0.0 copy-done.3
  148.5 0.1 fusion.38
  148.6 0.0 copy-done
  148.6 0.0 copy-start.4
  148.7 0.5 fusion.41
  149.1 0.0 copy-done.2
  149.2 0.1 add_dynamic-update-slice_fusion
  149.3 40.4 %all-reduce.1 = bf16[256,2048]{1,0:T(8,128)(2,1)} all-reduce(f32[256,2048]{1,0:T(8,128)S(1)} %add_dynamic-update-slice_fusion), channel_id=1, replica_groups=mesh['sp'=8,'tp'=4] {'tp'}, use_global_device_ids=true, to_apply=%region_6.7 | all-reduce | flops 524288 | bytes 3145728 | tf_op jit(solution)/shard_map/psum | solution.py:89
  189.7 1.5 fusion.29
  191.2 0.0 all-gather.3.cloned.1.call-done
  191.2 78.2 %all-gather.5.cloned.1.call-done = bf16[2048,2048]{1,0:T(8,128)(2,1)} async-done(((bf16[2048,256]{1,0:T(8,128)(2,1)}), bf16[2048,2048]{1,0:T(8,128)(2,1)}) %all-gather.5.cloned.1.call-update) | async-done | bytes 8388624 | tf_op jit(solution)/shard_map/all_gather | solution.py:102
  269.4 0.0 copy-done.4
  269.4 11.6 %convolution_convert_fusion = bf16[256,2048]{1,0:T(8,128)(2,1)} fusion(bf16[2048,2048]{1,0:T(8,128)(2,1)} %all-gather.5.cloned.1.call-done, bf16[2048,2048]{1,0:T(8,128)(2,1)} %all-gather.3.cloned.1.call-done, bf16[256,2048]{1,0:T(8,128)(2,1)} %all-reduce.1, f32[2048]{0:T(1024)S(1)} %copy-done.4, f32[256]{0:T(256)S(1)} %add_rsqrt_fusion.1), kind=kOutput, calls=%fused_computation.37 | convolution fusion | flops 4299161600 | bytes 18883584 | tf_op jit(solution)/shard_map/dot_general | solution.py:100
  281.1 0.0 reduce-scatter.2.cloned.1.call-update
  281.1 23.1 %reduce-scatter.2.cloned.1.call-done = bf16[256,512]{1,0:T(8,128)(2,1)} async-done(((bf16[256,2048]{1,0:T(8,128)(2,1)}), bf16[256,512]{1,0:T(8,128)(2,1)}) %reduce-scatter.2.cloned.1.call-update) | async-done | bytes 262160 | tf_op jit(solution)/shard_map/reduce_scatter | solution.py:105
  304.2 1.8 add_convert_fusion
  (11 shorter events, 0.1 us)
Async XLA Ops:
  6.5 142.1 %copy-start = (bf16[256,2048]{1,0:T(8,128)(2,1)S(1)}, bf16[256,2048]{1,0:T(8,128)(2,1)}, u32[]{:S(2)}) copy-start(bf16[256,2048]{1,0:T(8,128)(2,1)} %param.18) | copy-start | bytes 3145732
  6.5 184.7 %all-gather.3.cloned.1.call-start = ((), (), s32[]{:S(2)}) async-start(), calls=%async_computation.1 | async-start | bytes 9437184 | tf_op jit(solution)/shard_map/all_gather | solution.py:96
  7.3 262.1 %all-gather.5.cloned.1.call-start = ((), (), s32[]{:S(2)}) async-start(), calls=%async_computation.2 | async-start | bytes 9437184 | tf_op jit(solution)/shard_map/all_gather | solution.py:102
  8.0 296.2 %reduce-scatter.2.cloned.1.call-start = ((), (), s32[]{:S(2)}) async-start(), calls=%async_computation.3 | async-start | bytes 1310720 | tf_op jit(solution)/shard_map/reduce_scatter | solution.py:105
  99.9 48.6 %copy-start.3 = (f32[256]{0:T(256)S(1)}, f32[256]{0:T(256)}, u32[]{:S(2)}) copy-start(f32[256]{0:T(256)} %param.17) | copy-start | bytes 3076
  127.0 1.9 copy-start.1
  148.2 1.0 copy-start.2
  148.6 120.8 %copy-start.4 = (f32[2048]{0:T(1024)S(1)}, f32[2048]{0:T(1024)}, u32[]{:S(2)}) copy-start(f32[2048]{0:T(1024)} %param.19) | copy-start | bytes 24580
Sparse Core Ops, SparseCore 0:
  9.5 134.2 all-gather.2
  145.8 123.5 all-gather.4
  281.2 22.9 reduce-scatter.1
where the time goes:
time: 313 us
  blocking collectives  131 us (42%)
  waiting for transfers between devices  103 us (33%)
  matrix products  25.2 us (8%)
  local copies, waits for them, and re-layouts  20.1 us (6%)
  other arithmetic  19.6 us (6%)
  between operations  13.2 us (4%)
    all_gather x1, waiting for transfers between devices, body(): lax.all_gather(down_weight, 'sp', axis=1, tiled=True)  78.2 us
    psum x1, blocking collectives, body(): hidden_whole = lax.psum(partial_value, 'tp').astype(jnp.bfloat16)  40.4 us
    all_gather x1, blocking collectives, body(): lax.all_gather(key_rows, 'sp', axis=0, tiled=True)  35.3 us
    all_gather x1, blocking collectives, body(): lax.all_gather(value_rows, 'sp', axis=0, tiled=True)  33.5 us
    reduce_scatter x1, waiting for transfers between devices, body(): lax.psum_scatter(expanded.astype(jnp.bfloat16), 'tp', scatter_dimension=1...  23.1 us
    all_gather x1, blocking collectives, body(): lax.all_gather(break_shift, 'sp', axis=1, tiled=True)  22 us
    another operation x6, local copies, waits for them, and re-layouts  14.1 us
    dot_general x1, matrix products, body(): jnp.dot(activated, lax.all_gather(down_weight, 'sp', axis=1, tiled=True),...  11.6 us
  transfers between devices with their start and end apart: 3, of which 2 were waited for; matrix products, arithmetic and copies ran while one was open for 16% of the time, Pallas kernels for 0%

commit v1 on v0

--- a/solution.py
+++ b/solution.py
@@ -5,6 +5,11 @@
 
 HEAD_DIM = 128
 eps = 1e-06
+
+
+def add_all(block, name):
+    parts = lax.all_gather(block, name)
+    return jnp.sum(parts, axis=0)
 
 
 def stick_attention(queries, key_all, value_all, shift_all, first_pos, key_block):
@@ -86,7 +91,7 @@
         partial_value, column_start, column_count, 1
     ) + residual.astype(jnp.float32)
     partial_value = lax.dynamic_update_slice_in_dim(partial_value, own_part, column_start, 1)
-    hidden_whole = lax.psum(partial_value, "tp").astype(jnp.bfloat16)
+    hidden_whole = add_all(partial_value, "tp").astype(jnp.bfloat16)
     widened = hidden_whole.astype(jnp.float32)
     inverse = lax.rsqrt(jnp.mean(widened * widened, axis=1, keepdims=True) + eps)
     mlp_in = (widened * inverse * mlp_gain).astype(jnp.bfloat16)

time: 313 us -> 496 us (1.58)
  waiting for transfers between devices: 103 us -> 326 us
  blocking collectives: 131 us -> 85.9 us
    all_gather x1, waiting for transfers between devices: 0.02 us -> 122 us  [body(): lax.all_gather(up_weight, 'sp', axis=0, tiled=True)]
    all_gather x0 -> x1, waiting for transfers between devices: none -> 54.2 us  [add_all(): parts = lax.all_gather(block, name)]
    all_gather x1, waiting for transfers between devices: 78.2 us -> 125 us  [body(): lax.all_gather(down_weight, 'sp', axis=1, tiled=True)]
    psum x1 -> x0, blocking collectives: 40.4 us -> none  [body(): hidden_whole = lax.psum(partial_value, 'tp').astype(jnp.bfloat16)]
  transfers between devices with their start and end apart: 3 -> 4, of which waited for: 2 -> 4; matrix products, arithmetic and copies ran while one was open for 16% -> 1% of each run, Pallas kernels for 0% -> 0%
where the time goes in v1:
time: 496 us; the launch traced here: 495 us
  waiting for transfers between devices  326 us (66%)
  blocking collectives  85.9 us (17%)
  matrix products  24.8 us (5%)
  other arithmetic  23.6 us (5%)
  local copies, waits for them, and re-layouts  21.5 us (4%)
  between operations  13.2 us (3%)
    all_gather x1, waiting for transfers between devices, body(): lax.all_gather(down_weight, 'sp', axis=1, tiled=True)  125 us
    all_gather x1, waiting for transfers between devices, body(): lax.all_gather(up_weight, 'sp', axis=0, tiled=True)  122 us
    all_gather x1, waiting for transfers between devices, add_all(): parts = lax.all_gather(block, name)  54.2 us
    all_gather x1, blocking collectives, body(): lax.all_gather(key_rows, 'sp', axis=0, tiled=True)  33.4 us
    all_gather x1, blocking collectives, body(): lax.all_gather(value_rows, 'sp', axis=0, tiled=True)  31.4 us
    reduce_scatter x1, waiting for transfers between devices, body(): lax.psum_scatter(expanded.astype(jnp.bfloat16), 'tp', scatter_dimension=1...  23.1 us
    all_gather x1, blocking collectives, body(): lax.all_gather(break_shift, 'sp', axis=1, tiled=True)  21.1 us
    another operation x6, local copies, waits for them, and re-layouts  14.1 us
  transfers between devices with their start and end apart: 4, of which 4 were waited for; matrix products, arithmetic and copies ran while one was open for 1% of the time, Pallas kernels for 0%

profile of v1, /device:TPU:0, one launch (start us, length us, event | category | flops | bytes accessed | tf_op | source)
XLA Modules:
  0.0 495.2 jit_solution(9299757350554008745)
XLA Ops:
  6.5 0.0 copy-start
  6.5 0.0 all-gather.4.cloned.1.call-start
  6.5 33.4 %all_gather.23 = bf16[2048,128]{1,0:T(8,128)(2,1)S(1)} all-gather(bf16[256,128]{1,0:T(8,128)(2,1)} %param.14), channel_id=1, replica_groups=mesh['sp'=8,'tp'=4] {'sp'}, dimensions={0}, use_global_device_ids=true | all-gather | bytes 589824 | tf_op jit(solution)/shard_map/all_gather | solution.py:76
  39.9 31.4 %all_gather.25 = bf16[2048,128]{1,0:T(8,128)(2,1)S(1)} all-gather(bf16[256,128]{1,0:T(8,128)(2,1)} %param.15), channel_id=1, replica_groups=mesh['sp'=8,'tp'=4] {'sp'}, dimensions={0}, use_global_device_ids=true | all-gather | bytes 589824 | tf_op jit(solution)/shard_map/all_gather | solution.py:77
  71.3 0.9 reshape.146
  72.3 21.1 %all_gather.24 = bf16[1,2048]{1,0:T(2,128)(2,1)S(1)} all-gather(bf16[1,256]{1,0:T(2,128)(2,1)} %param.16), channel_id=1, replica_groups=mesh['sp'=8,'tp'=4] {'sp'}, dimensions={1}, use_global_device_ids=true | all-gather | bytes 4608 | tf_op jit(solution)/shard_map/all_gather | solution.py:78
  93.5 0.0 copy-start.3
  93.5 48.3 %while.15 = (s32[]{:T(128)}, f32[1,512,128]{2,1,0:T(8,128)S(1)}, f32[1,512]{1,0:T(1,128)S(1)}, s32[]{:T(128)}, s32[]{:T(128)}, /*index=5*/bf16[1,512,128]{2,1,0:...) while((s32[]{:T(128)}, f32[1,512,128]{2,1,0:T(8,128)S(1)}, ...), condition=%wide.region_4.5_spmd.clone, body=%wide.region_0.4_spmd.clone.sunk | while | flops 709041152 | bytes 81762496 | solution.py:56
  93.5 2.6 fusion.64
  96.2 5.0 %fusion.66 = (f32[512]{0:T(512)S(1)}, f32[64,8,16,128]{3,1,2,0:T(8,128)S(1)}) fusion(f32[2048]{0:T(1024)S(1)} %bitcast.102, f32[512,2048]{1,0:T(8,128)} %fusion.64, s32[512]{0:T(512)S(1)} %fusion.65, s32[2048]{0:T(1024)S(1)} %iota_add_fusion.2), kind=kLoop, calls=%fused_computation.30.clone.1 | loop fusion | flops 12582400 | bytes 8409088 | tf_op jit(solution)/shard_map/while/body/reduce_sum | solution.py:50
  101.2 2.9 copy.52
  104.1 5.6 %copy.53 = f32[1,512,16,128]{1,2,3,0:T(8,128)} copy(f32[1,512,16,128]{3,2,1,0:T(8,128)} %bitcast.95) | data formatting | bytes 8388608 | tf_op jit(solution)/shard_map/reshape.114
  109.7 10.8 %fusion.67 = f32[1,512,16,128]{1,2,3,0:T(8,128)S(1)} fusion(f32[1,512,16,128]{1,2,3,0:T(8,128)} %copy.53), kind=kOutput, calls=%fused_computation.52.clone.1 | output fusion | flops 133169152 | bytes 8388608 | tf_op jit(solution)/shard_map/reduce-window.4
  120.5 0.0 copy-start.1
  120.5 1.9 copy-done.1
  122.5 0.1 reduce-window.20
  122.6 0.1 copy.54
  122.7 2.6 broadcast.100
  125.3 5.8 %copy.55 = f32[1,512,16,128]{3,2,1,0:T(8,128)} copy(f32[1,512,16,128]{1,2,3,0:T(8,128)} %copy-done.1) | data formatting | bytes 8388608 | tf_op jit(solution)/shard_map/reduce-window.4
  131.1 10.4 %fusion.68 = f32[1,512,128]{2,1,0:T(8,128)S(1)} fusion(f32[1,512,128]{2,1,0:T(8,128)S(1)} %get-tuple-element.245, bf16[2048,128]{1,0:T(8,128)(2,1)S(1)} %get-tuple-element.265, f32[64,8,16,128]{3,2,1,0:T(8,128)} %bitcast.96, f32[64,8,16,128]{3,2,1,0:T(8,128)} %bitcast.97, f32[512,2048]{1,0:T(8,128)} %fusion.64, f32[512]{0:T(512)S(1)} %bitcast.105, ...), kind=kOutput, calls=%fused_computation.16.clone.1 | convolution fusion | flops 294715392 | bytes 13651968 | tf_op jit(solution)/shard_map/while/body/grk,kgd->grd/dot_general | solution.py:47
  141.7 0.1 copy.28
  141.9 0.0 copy-start.2
  141.9 0.1 multiply_reduce_fusion
  142.0 0.0 copy-done.3
  142.1 0.1 fusion.38
  142.2 0.0 copy-done
  142.2 0.5 fusion.41
  142.6 1.4 copy.65
  144.0 0.0 copy-done.2
  144.0 0.9 bitcast_dynamic-update-slice_fusion
  144.9 0.0 all-gather.4.cloned.1.call-update
  145.0 0.0 all-gather.6.cloned.1.call-start
  145.0 0.7 all-gather.6.cloned.1.call-update
  145.7 0.0 all-gather.8.cloned.1.call-start
  145.8 0.7 all-gather.8.cloned.1.call-update
  146.5 0.0 copy-start.4
  146.5 0.0 reduce-scatter.2.cloned.1.call-start
  146.5 54.2 %all-gather.4.cloned.1.call-done = f32[4,256,2048]{2,1,0:T(8,128)} async-done(((f32[1,256,2048]{2,1,0:T(8,128)}), f32[4,256,2048]{2,1,0:T(8,128)}) %all-gather.4.cloned.1.call-update) | async-done | bytes 8388624 | tf_op jit(solution)/shard_map/all_gather | solution.py:11
  200.7 4.4 reduce_sum.39
  205.1 0.3 fusion.29
  205.4 121.9 %all-gather.6.cloned.1.call-done = bf16[2048,2048]{1,0:T(8,128)(2,1)} async-done(((bf16[256,2048]{1,0:T(8,128)(2,1)}), bf16[2048,2048]{1,0:T(8,128)(2,1)}) %all-gather.6.cloned.1.call-update) | async-done | bytes 8388624 | tf_op jit(solution)/shard_map/all_gather | solution.py:101
  327.3 125.2 %all-gather.8.cloned.1.call-done = bf16[2048,2048]{1,0:T(8,128)(2,1)} async-done(((bf16[2048,256]{1,0:T(8,128)(2,1)}), bf16[2048,2048]{1,0:T(8,128)(2,1)}) %all-gather.8.cloned.1.call-update) | async-done | bytes 8388624 | tf_op jit(solution)/shard_map/all_gather | solution.py:107
  452.5 0.0 copy-done.4
  452.5 11.3 %convolution_convert_fusion = bf16[256,2048]{1,0:T(8,128)(2,1)} fusion(bf16[2048,2048]{1,0:T(8,128)(2,1)} %all-gather.8.cloned.1.call-done, bf16[2048,2048]{1,0:T(8,128)(2,1)} %all-gather.6.cloned.1.call-done, bf16[256,2048]{1,0:T(8,128)(2,1)S(1)} %reduce_sum.39, f32[2048]{0:T(1024)S(1)} %copy-done.4, f32[256]{0:T(256)S(1)} %add_rsqrt_fusion.1), kind=kOutput, calls=%fused_computation.37 | convolution fusion | flops 4299161600 | bytes 18883584 | tf_op jit(solution)/shard_map/dot_general | solution.py:105
  463.8 0.0 reduce-scatter.2.cloned.1.call-update
  463.8 23.1 %reduce-scatter.2.cloned.1.call-done = bf16[256,512]{1,0:T(8,128)(2,1)} async-done(((bf16[256,2048]{1,0:T(8,128)(2,1)}), bf16[256,512]{1,0:T(8,128)(2,1)}) %reduce-scatter.2.cloned.1.call-update) | async-done | bytes 262160 | tf_op jit(solution)/shard_map/reduce_scatter | solution.py:110
  487.0 1.7 add_convert_fusion
  (11 shorter events, 0.1 us)
Async XLA Ops:
  6.5 135.6 %copy-start = (bf16[256,2048]{1,0:T(8,128)(2,1)S(1)}, bf16[256,2048]{1,0:T(8,128)(2,1)}, u32[]{:S(2)}) copy-start(bf16[256,2048]{1,0:T(8,128)(2,1)} %param.18) | copy-start | bytes 3145732
  6.5 194.1 %all-gather.4.cloned.1.call-start = ((), (), s32[]{:S(2)}) async-start(), calls=%async_computation.1 | async-start | bytes 10485760 | tf_op jit(solution)/shard_map/all_gather | solution.py:11
  93.5 48.6 %copy-start.3 = (f32[256]{0:T(256)S(1)}, f32[256]{0:T(256)}, u32[]{:S(2)}) copy-start(f32[256]{0:T(256)} %param.17) | copy-start | bytes 3076
  120.5 2.0 copy-start.1
  141.9 2.2 copy-start.2
  145.0 182.3 %all-gather.6.cloned.1.call-start = ((), (), s32[]{:S(2)}) async-start(), calls=%async_computation.2 | async-start | bytes 9437184 | tf_op jit(solution)/shard_map/all_gather | solution.py:101
  145.7 306.8 %all-gather.8.cloned.1.call-start = ((), (), s32[]{:S(2)}) async-start(), calls=%async_computation.3 | async-start | bytes 9437184 | tf_op jit(solution)/shard_map/all_gather | solution.py:107
  146.5 306.1 %copy-start.4 = (f32[2048]{0:T(1024)S(1)}, f32[2048]{0:T(1024)}, u32[]{:S(2)}) copy-start(f32[2048]{0:T(1024)} %param.19) | copy-start | bytes 24580
  146.5 340.5 %reduce-scatter.2.cloned.1.call-start = ((), (), s32[]{:S(2)}) async-start(), calls=%async_computation.4 | async-start | bytes 1310720 | tf_op jit(solution)/shard_map/reduce_scatter | solution.py:110
Sparse Core Ops, SparseCore 0:
  145.1 55.5 all-gather.3
  202.8 124.4 all-gather.5
  329.4 123.1 all-gather.7
  464.0 22.9 reduce-scatter.1
